TPU v7x, 32 devices: a whole 2x2x4 slice. The times are simulated.
32 devices in a mesh: ep: 8 (over z, x), tp: 4 (over y, core).
Axes of the slice: x: 2, y: 2, z: 4, core: 2. Of those that a mesh axis runs over, the one named last changes fastest.
Arguments:
- queries: bfloat16 [2048, 4096], P('ep', 'tp'), may hold values from -6 to 6
- key_rows: bfloat16 [2048, 4096], P('ep', 'tp'), may hold values from -6 to 6
- value_rows: bfloat16 [2048, 4096], P('ep', 'tp'), may hold values from -6 to 6
- lambdas: float32 [16], P('tp'), may hold values from 0.3 to 0.8
- head_gain: float32 [256], replicated, may hold values from 0.1 to 1.9
- out_proj: bfloat16 [4096, 2048], P('tp'), may hold values from -0.09375 to 0.09375
- moe_input: bfloat16 [1024, 2048], P('ep'), may hold values from -6 to 6
- moe_gain: float32 [2048], replicated, may hold values from 0.1 to 1.9
- routes: int32 [1024, 2], P('ep'), may hold values from 0 to 7, all different within a row; in each aligned block of 32 rows (0 to 31, 32 to 63, ...) at most 16 rows name the same one
- route_weights: float32 [1024, 2], P('ep'), may hold values from 0.2 to 1.2
- expert_gate: bfloat16 [8, 2048, 1024], P('ep', None, 'tp'), may hold values from -0.125 to 0.125
- expert_up: bfloat16 [8, 2048, 1024], P('ep', None, 'tp'), may hold values from -0.125 to 0.125
- expert_down: bfloat16 [8, 1024, 2048], P('ep', 'tp'), may hold values from -0.1875 to 0.1875
- shared_gate: bfloat16 [2048, 1024], P(None, 'tp'), may hold values from -0.125 to 0.125
- shared_up: bfloat16 [2048, 1024], P(None, 'tp'), may hold values from -0.125 to 0.125
- shared_down: bfloat16 [1024, 2048], P('tp'), may hold values from -0.1875 to 0.1875
Outputs:
- mixer_out: bfloat16 [2048, 2048], P(('ep', 'tp'))
- moe_out: bfloat16 [1024, 2048], P(('ep', 'tp'))
Inputs may be any that keep to these rules, and one draw needn't show every extreme that they name: `routes`: each row names 2 different experts. The rows of one index of ep fall into 4 aligned blocks of equal size; no expert is named by more than 16 rows of one block, and in every draw some expert is named by exactly 16 rows of some block.
All inputs are finite; a program needn't handle non-finite values.
Results may differ from a plain program's by a relative error of at most 0.02.
Values may be sent and summed in bfloat16 or wider, within the bound.
No kernel may reach another device: no remote copies, remote signals or barrier semaphores. Data moves between devices by JAX's collectives and lax.ppermute only.
A program may use at most 128 MiB of HBM per device.

v0:
```python
import jax
import jax.numpy as jnp
from jax import lax
from jax.sharding import PartitionSpec as P

theta_base = 500000.0
norm_eps = 1e-06
head_eps = 1e-05


def rotate(matrix, positions, head_dim):
    row_count = matrix.shape[0]
    shaped = matrix.reshape(row_count, -1, head_dim).astype(jnp.float32)
    half_dim = head_dim // 2
    frequency = jnp.power(theta_base, -jnp.arange(half_dim, dtype=jnp.float32) * 2.0 / head_dim)
    angles = positions.astype(jnp.float32)[:, None] * frequency[None, :]
    cosine = jnp.cos(angles)[:, None, :]
    sines = jnp.sin(angles)[:, None, :]
    front_half = shaped[..., :half_dim]
    second = shaped[..., half_dim:]
    turned = jnp.concatenate(
        [front_half * cosine - second * sines, second * cosine + front_half * sines], axis=-1
    )
    return turned.reshape(matrix.shape).astype(jnp.bfloat16)


def rms_rows(values, gain):
    widened = values.astype(jnp.float32)
    mean_square = jnp.mean(widened * widened, axis=-1, keepdims=True)
    return (widened * lax.rsqrt(mean_square + norm_eps) * gain).astype(jnp.bfloat16)


def gated_hidden(rows_in, gate_weight, up_weight):
    gate_part = jnp.dot(rows_in, gate_weight, preferred_element_type=jnp.float32)
    up_part = jnp.dot(rows_in, up_weight, preferred_element_type=jnp.float32)
    return (jax.nn.silu(gate_part) * up_part).astype(jnp.bfloat16)


def slot_hidden(slot_rows, gate_weight, up_weight):
    gate_part = jnp.einsum(
        "xnsd,xdf->xnsf", slot_rows, gate_weight, preferred_element_type=jnp.float32
    )
    up_part = jnp.einsum("xnsd,xdf->xnsf", slot_rows, up_weight, preferred_element_type=jnp.float32)
    return (jax.nn.silu(gate_part) * up_part).astype(jnp.bfloat16)


def key_block_size(piece_rows):
    for candidate in (1024, 512):
        return candidate
    return piece_rows


def fold_keys(state_in, pieces, rot_query, head_count, head_dim):
    keys_piece, values_piece = pieces
    piece_rows = keys_piece.shape[0]
    block_rows = key_block_size(piece_rows)
    block_count = piece_rows // block_rows
    query_view = rot_query.reshape(rot_query.shape[0], head_count, 2, head_dim)
    score_scale = head_dim ** (-0.5)

    def one_block(running, key_block):
        running_max, denominator, numerator = running
        key_view = key_block[0].reshape(block_rows, head_count, 2, head_dim)
        value_view = key_block[1].reshape(block_rows, head_count, 2 * head_dim)
        scores = (
            jnp.einsum("qhmd,khmd->hmqk", query_view, key_view, preferred_element_type=jnp.float32)
            * score_scale
        )
        newest = jnp.maximum(running_max, jnp.max(scores, axis=-1))
        weights = jnp.exp(scores - newest[..., None])
        shrink = jnp.exp(running_max - newest)
        denominator = denominator * shrink + jnp.sum(weights, axis=-1)
        weighted = jnp.einsum(
            "hmqk,khe->hmqe",
            weights.astype(jnp.bfloat16),
            value_view,
            preferred_element_type=jnp.float32,
        )
        numerator = numerator * shrink[..., None] + weighted
        return ((newest, denominator, numerator), None)

    blocks = (
        keys_piece.reshape(block_count, block_rows, -1),
        values_piece.reshape(block_count, block_rows, -1),
    )
    result, _ = lax.scan(one_block, state_in, blocks)
    return result


def slot_table(route_block, expert_count, capacity):
    flat_routes = route_block.reshape(-1)
    route_total = flat_routes.shape[0]
    top_count = route_block.shape[1]
    experts_iota = jnp.arange(expert_count, dtype=jnp.int32)
    onehot = (flat_routes[:, None] == experts_iota[None, :]).astype(jnp.int32)
    before = jnp.cumsum(onehot, axis=0) - onehot
    slot_rank = jnp.sum(before * onehot, axis=1)
    slot_iota = jnp.arange(capacity, dtype=jnp.int32)
    matches = (flat_routes[None, None, :] == experts_iota[:, None, None]) & (
        slot_rank[None, None, :] == slot_iota[None, :, None]
    )
    source_row = jnp.arange(route_total, dtype=jnp.int32) // top_count
    source = jnp.sum(jnp.where(matches, source_row[None, None, :], 0), axis=2)
    filled = jnp.any(matches, axis=2)
    return (source, filled, slot_rank.reshape(route_block.shape))


def fill_slots(rows_src, source, filled):
    taken = jnp.take(rows_src, source.reshape(-1), axis=0).reshape(
        source.shape + (rows_src.shape[1],)
    )
    return jnp.where(filled[..., None], taken, jnp.zeros_like(taken))


def local(
    queries,
    key_rows,
    value_rows,
    lambdas,
    head_gain,
    out_proj,
    moe_input,
    moe_gain,
    routes,
    route_weights,
    expert_gate,
    expert_up,
    expert_down,
    shared_gate,
    shared_up,
    shared_down,
):
    query_rows = queries.shape[0]
    head_count = lambdas.shape[0]
    head_dim = queries.shape[1] // (2 * head_count)
    tp_count = lax.axis_size("tp")
    ep_count = lax.axis_size("ep")
    tp_place = lax.axis_index("tp")
    ep_place = lax.axis_index("ep")
    positions = ep_place * query_rows + jnp.arange(query_rows, dtype=jnp.int32)
    rot_query = rotate(queries, positions, head_dim)
    rot_keys = rotate(key_rows, positions, head_dim)
    initial = (
        jnp.full((head_count, 2, query_rows), -1e30, jnp.float32),
        jnp.zeros((head_count, 2, query_rows), jnp.float32),
        jnp.zeros((head_count, 2, query_rows, 2 * head_dim), jnp.float32),
    )
    running_max, denominator, numerator = fold_keys(
        initial,
        (
            lax.all_gather(rot_keys, "ep", axis=0, tiled=True),
            lax.all_gather(value_rows, "ep", axis=0, tiled=True),
        ),
        rot_query,
        head_count,
        head_dim,
    )
    ratio = numerator / denominator[..., None]
    mixed_heads = ratio[:, 0] - lambdas[:, None, None] * ratio[:, 1]
    mean_square = jnp.mean(mixed_heads * mixed_heads, axis=-1, keepdims=True)
    normed_heads = (mixed_heads * lax.rsqrt(mean_square + head_eps) * head_gain).astype(
        jnp.bfloat16
    )
    head_out = jnp.transpose(normed_heads, (1, 0, 2)).reshape(query_rows, head_count * 2 * head_dim)
    normed = rms_rows(moe_input, moe_gain)
    shared_hidden = gated_hidden(normed, shared_gate, shared_up)
    batch_rows = moe_input.shape[0]
    top_count = routes.shape[1]
    own_rows = batch_rows // tp_count
    local_experts = expert_gate.shape[0]
    expert_count = local_experts * ep_count
    capacity = (2 * own_rows * top_count + expert_count - 1) // expert_count
    own_routes = lax.dynamic_slice_in_dim(routes, tp_place * own_rows, own_rows, 0)
    own_weights = lax.dynamic_slice_in_dim(route_weights, tp_place * own_rows, own_rows, 0)
    own_source, own_filled, own_rank = slot_table(own_routes, expert_count, capacity)
    own_normed = lax.dynamic_slice_in_dim(normed, tp_place * own_rows, own_rows, 0)
    outgoing = fill_slots(own_normed, own_source, own_filled)
    arrived = lax.all_to_all(outgoing[:, None], "ep", split_axis=0, concat_axis=2, tiled=True)
    hidden = slot_hidden(lax.all_gather(arrived, "tp", axis=1, tiled=True), expert_gate, expert_up)
    slot_rows = local_experts * ep_count * capacity
    mixer_share = query_rows // tp_count
    expert_share = own_rows + slot_rows
    block_count = lax.axis_size("tp") * mixer_share // mixer_share
    product = jnp.dot(head_out, out_proj, preferred_element_type=jnp.float32)
    mixer_out = lax.psum_scatter(
        product.reshape(block_count, mixer_share, -1)
        .reshape(lax.axis_size("tp") * mixer_share, -1)
        .astype(jnp.bfloat16),
        "tp",
        scatter_dimension=0,
        tiled=True,
    )
    block_count = lax.axis_size("tp") * expert_share // expert_share
    shared_part = jnp.dot(shared_hidden, shared_down, preferred_element_type=jnp.float32).reshape(
        block_count, own_rows, -1
    )
    routed_part = jnp.einsum(
        "xnsf,xfd->nxsd", hidden, expert_down, preferred_element_type=jnp.float32
    )
    routed_part = routed_part.reshape(block_count, slot_rows, -1)
    expert_sum = lax.psum_scatter(
        jnp.concatenate([shared_part, routed_part], axis=1)
        .reshape(lax.axis_size("tp") * expert_share, -1)
        .astype(jnp.bfloat16),
        "tp",
        scatter_dimension=0,
        tiled=True,
    ).astype(jnp.float32)
    shared_sum = expert_sum[:own_rows]
    routed = (
        expert_sum[own_rows:].reshape(local_experts, ep_count * capacity, -1).astype(jnp.bfloat16)
    )
    returned = lax.all_to_all(routed, "ep", split_axis=1, concat_axis=0, tiled=True)
    flat_index = (own_routes * capacity + own_rank).reshape(-1)
    picked = jnp.take(returned.reshape(expert_count * capacity, -1), flat_index, axis=0).reshape(
        own_rows, top_count, -1
    )
    combined = shared_sum + jnp.sum(own_weights[..., None] * picked.astype(jnp.float32), axis=1)
    return (mixer_out, combined.astype(jnp.bfloat16))


def solution(mesh):
    in_specs = (
        P("ep", "tp"),
        P("ep", "tp"),
        P("ep", "tp"),
        P("tp"),
        P(),
        P("tp", None),
        P("ep", None),
        P(),
        P("ep", None),
        P("ep", None),
        P("ep", None, "tp"),
        P("ep", None, "tp"),
        P("ep", "tp", None),
        P(None, "tp"),
        P(None, "tp"),
        P("tp", None),
    )
    out_specs = (P(("ep", "tp"), None), P(("ep", "tp"), None))
    return jax.shard_map(local, mesh=mesh, in_specs=in_specs, out_specs=out_specs, check_vma=False)
```

profile of v0, /device:TPU:0, one launch (start us, length us, event | category | flops | bytes accessed | tf_op | source)
XLA Modules:
  0.0 299.0 jit_solution(7164082927943811089)
XLA Ops:
  12.8 21.7 %all_to_all.21 = bf16[8,1,16,2048]{3,2,1,0:T(8,128)(2,1)} all-to-all(bf16[8,1,16,2048]{3,2,1,0:T(8,128)(2,1)S(1)} %select_select_fusion), channel_id=1, replica_groups=mesh['ep'=8,'tp'=4] {'ep'}, dimensions={0} | all-to-all | bytes 1048576 | tf_op jit(solution)/shard_map/all_to_all | solution.py:178
  34.8 2.2 copy.96
  37.4 2.2 subtract_convert_fusion
  43.3 1.5 fusion.53
  44.9 2.0 convolution_convert_fusion.2
  46.9 9.4 %all-gather.8.cloned.1.call-done = bf16[1,4,128,2048]{3,2,0,1:T(8,128)(2,1)} async-done(((bf16[1,1,128,2048]{3,2,0,1:T(8,128)(2,1)}), bf16[1,4,128,2048]{3,2,0,1:T(8,128)(2,1)}) %all-gather.8.cloned.1.call-update) | async-done | bytes 2097168 | tf_op jit(solution)/shard_map/all_gather | solution.py:179
  56.3 2.6 fusion.15
  58.9 5.2 %convolution_convert_fusion = bf16[4,128,2048]{2,1,0:T(8,128)(2,1)} fusion(bf16[1,4,128,2048]{3,2,0,1:T(8,128)(2,1)} %all-gather.8.cloned.1.call-done, bf16[1,256,2048]{2,1,0:T(8,128)(2,1)S(1)} %copy-done, bf16[1,2048,256]{2,1,0:T(8,128)(2,1)S(1)} %copy-done.12, f32[4,128,256]{2,1,0:T(8,128)S(1)} %fusion.15), kind=kOutput, calls=%fused_computation.21 | convolution fusion | flops 1075576832 | bytes 6815744 | tf_op jit(solution)/shard_map/xnsf,xfd->nxsd/dot_general | solution.py:197
  64.2 3.5 %pad_maximum_fusion = bf16[4,160,2048]{2,1,0:T(8,128)(2,1)} fusion(bf16[4,128,2048]{2,1,0:T(8,128)(2,1)} %convolution_convert_fusion, bf16[4,32,2048]{2,1,0:T(8,128)(2,1)S(1)} %bitcast.130), kind=kLoop, calls=%fused_computation.22 | loop fusion | flops 5242880 | bytes 5242880 | tf_op jit(solution)/shard_map/concatenate | solution.py:202
  67.9 65.1 %all-gather.4.cloned.1.call-done = bf16[2048,1024]{0,1:T(8,128)(2,1)} async-done(((bf16[256,1024]{0,1:T(8,128)(2,1)}), bf16[2048,1024]{0,1:T(8,128)(2,1)}) %all-gather.4.cloned.1.call-update) | async-done | bytes 4194320 | tf_op jit(solution)/shard_map/all_gather | solution.py:151
  133.0 4.7 %copy.122 = bf16[128,2,8,1024]{3,2,0,1:T(8,128)(2,1)} copy(bf16[128,2,8,1024]{3,2,1,0:T(8,128)(2,1)} %bitcast.128) | data formatting | bytes 8388608 | tf_op jit(solution)/shard_map/reshape | solution.py:83
  137.7 68.5 %all-gather.6.cloned.1.call-done = bf16[2048,1024]{1,0:T(8,128)(2,1)} async-done(((bf16[256,1024]{1,0:T(8,128)(2,1)}), bf16[2048,1024]{1,0:T(8,128)(2,1)}) %all-gather.6.cloned.1.call-update) | async-done | bytes 4194320 | tf_op jit(solution)/shard_map/all_gather | solution.py:152
  206.2 48.7 %while.15 = (s32[]{:T(128)}, f32[4,2,256]{2,1,0:T(2,128)S(1)}, f32[4,2,256]{2,1,0:T(2,128)S(1)}, f32[4,2,256,256]{3,2,1,0:T(8,128)}, bf16[2,1024,1024]{1,2,0:T(8...) while((s32[]{:T(128)}, f32[4,2,256]{2,1,0:T(2,128)S(1)}, ...), condition=%wide.region_3.4_spmd.clone, body=%wide.region_0.3_spmd.clone.sunk | while | flops 1628973056 | bytes 63570068 | solution.py:86
  206.2 1.8 constant_dynamic-slice_fusion.7
  207.9 5.7 %bitcast_reduce_fusion.2 = (f32[4,2,256]{2,1,0:T(2,128)S(1)}, f32[4,2,1024,256]{3,2,1,0:T(8,128)}) fusion(bf16[1024,4,2,128]{0,3,2,1:T(8,128)(2,1)S(1)} %bitcast.119, bf16[256,4,2,128]{3,0,2,1:T(8,128)(2,1)} %get-tuple-element.210), kind=kOutput, calls=%fused_computation.3.clone.1 | convolution fusion | flops 541063168 | bytes 11018240 | tf_op jit(solution)/shard_map/while/body/eval_jaxpr/qhmd,khmd->hmqk/dot_general | solution.py:66
  213.6 5.7 %fusion.77 = f32[4,2,256]{2,1,0:T(2,128)S(1)} fusion(f32[4,2,1024,256]{3,2,1,0:T(8,128)} %get-tuple-element.184, f32[4,2,256]{2,1,0:T(2,128)S(1)} %fusion.76), kind=kLoop, calls=%fused_computation.6.clone.1 | loop fusion | flops 6289408 | bytes 8404992 | tf_op jit(solution)/shard_map/while/body/eval_jaxpr/reduce_sum | solution.py:72
  219.3 1.5 constant_dynamic-slice_fusion.8
  220.9 2.9 copy.126
  223.7 7.0 %fusion.79 = f32[4,2,256,256]{3,2,1,0:T(8,128)} fusion(f32[4,2,256,256]{3,2,1,0:T(8,128)} %get-tuple-element.199, bf16[1024,4,256,1]{0,2,3,1:T(8,128)(2,1)S(1)} %bitcast.120, f32[4,2,1024,256]{3,2,1,0:T(8,128)} %get-tuple-element.184, f32[4,2,256]{2,1,0:T(2,128)S(1)} %fusion.76, f32[4,2,256]{2,1,0:T(2,128)S(1)} %get-tuple-element.186, pred[]{:T(512)S(6)} %compare.7), kind=kOutput, calls=%fused_computation.11.clone.1 | convolution fusion | flops 1081606144 | bytes 14696449 | tf_op jit(solution)/shard_map/while/body/eval_jaxpr/hmqk,khe->hmqe/dot_general | solution.py:73
  230.8 1.8 constant_dynamic-slice_fusion.7
  232.6 5.6 %bitcast_reduce_fusion.2 = (f32[4,2,256]{2,1,0:T(2,128)S(1)}, f32[4,2,1024,256]{3,2,1,0:T(8,128)}) fusion(bf16[1024,4,2,128]{0,3,2,1:T(8,128)(2,1)S(1)} %bitcast.119, bf16[256,4,2,128]{3,0,2,1:T(8,128)(2,1)} %get-tuple-element.210), kind=kOutput, calls=%fused_computation.3.clone.1 | convolution fusion | flops 541063168 | bytes 11018240 | tf_op jit(solution)/shard_map/while/body/eval_jaxpr/qhmd,khmd->hmqk/dot_general | solution.py:66
  238.2 4.9 %fusion.77 = f32[4,2,256]{2,1,0:T(2,128)S(1)} fusion(f32[4,2,1024,256]{3,2,1,0:T(8,128)} %get-tuple-element.184, f32[4,2,256]{2,1,0:T(2,128)S(1)} %fusion.76), kind=kLoop, calls=%fused_computation.6.clone.1 | loop fusion | flops 6289408 | bytes 8404992 | tf_op jit(solution)/shard_map/while/body/eval_jaxpr/reduce_sum | solution.py:72
  243.1 1.5 constant_dynamic-slice_fusion.8
  244.7 2.9 copy.126
  247.5 7.4 %fusion.79 = f32[4,2,256,256]{3,2,1,0:T(8,128)} fusion(f32[4,2,256,256]{3,2,1,0:T(8,128)} %get-tuple-element.199, bf16[1024,4,256,1]{0,2,3,1:T(8,128)(2,1)S(1)} %bitcast.120, f32[4,2,1024,256]{3,2,1,0:T(8,128)} %get-tuple-element.184, f32[4,2,256]{2,1,0:T(2,128)S(1)} %fusion.76, f32[4,2,256]{2,1,0:T(2,128)S(1)} %get-tuple-element.186, pred[]{:T(512)S(6)} %compare.7), kind=kOutput, calls=%fused_computation.11.clone.1 | convolution fusion | flops 1081606144 | bytes 14696449 | tf_op jit(solution)/shard_map/while/body/eval_jaxpr/hmqk,khe->hmqe/dot_general | solution.py:73
  254.9 2.1 copy.102
  259.9 2.3 convolution_convert_fusion.1
  264.7 3.7 %reduce = bf16[128,2048]{1,0:T(8,128)(2,1)S(1)} reduce(bf16[128,1,2048]{2,1,0:T(2,128)(2,1)S(1)} %bitcast.129, bf16[]{:T(256)} %broadcast.288), dimensions={1}, to_apply=%bitcast.102.reduce_sub_computation | reduce | bytes 1048578
  269.6 3.5 %all-to-all-start.1 = ((bf16[8,2,16384]{2,1,0:T(2,128)(2,1)}), bf16[8,2,16384]{2,1,0:T(2,128)(2,1)S(1)}, u32[]{:S(2)}, u32[]{:S(2)}) async-start(bf16[8,2,16384]{2,1,0:T(2,128)(2,1)} %reshape.361), calls=%async_computation.3 | async-start | bytes 1048576 | tf_op jit(solution)/shard_map/all_to_all | solution.py:213
  273.8 13.5 %all-to-all-done.1 = bf16[8,2,16384]{2,1,0:T(2,128)(2,1)S(1)} async-done(((bf16[8,2,16384]{2,1,0:T(2,128)(2,1)}), bf16[8,2,16384]{2,1,0:T(2,128)(2,1)S(1)}, u32[]{:S(2)}, u32[]{:S(2)}) %all-to-all-start.1) | async-done | bytes 524320 | tf_op jit(solution)/shard_map/all_to_all | solution.py:213
  289.2 1.7 multiply_reduce_fusion.1
  290.9 1.6 add_convert_fusion.2
  (100 shorter events, 19.1 us)
Async XLA Ops:
  7.2 51.7 %copy-start = (bf16[1,256,2048]{2,1,0:T(8,128)(2,1)S(1)}, bf16[1,256,2048]{2,1,0:T(8,128)(2,1)}, u32[]{:S(2)}) copy-start(bf16[1,256,2048]{2,1,0:T(8,128)(2,1)} %param.30) | copy-start | bytes 3145732
  7.2 49.2 %all-gather.8.cloned.1.call-start = ((), (), s32[]{:S(2)}) async-start(), calls=%async_computation.7 | async-start | bytes 2621440 | tf_op jit(solution)/shard_map/all_gather | solution.py:179
  8.6 1.8 copy-start.5
  12.7 22.0 %copy-start.4 = (bf16[256,1024]{1,0:T(8,128)(2,1)S(1)}, bf16[256,1024]{1,0:T(8,128)(2,1)}, u32[]{:S(2)}) copy-start(bf16[256,1024]{1,0:T(8,128)(2,1)} %param.18) | copy-start | bytes 1572868
  34.6 98.5 %all-gather.4.cloned.1.call-start = ((), (), s32[]{:S(2)}) async-start(), calls=%async_computation.4 | async-start | bytes 4718592 | tf_op jit(solution)/shard_map/all_gather | solution.py:151
  40.5 4.4 %copy-start.3 = (bf16[256,2048]{1,0:T(8,128)(2,1)S(1)}, bf16[256,2048]{1,0:T(8,128)(2,1)}, u32[]{:S(2)}) copy-start(bf16[256,2048]{1,0:T(8,128)(2,1)} %param.33) | copy-start | bytes 3145732
  40.5 165.7 %all-gather.6.cloned.1.call-start = ((), (), s32[]{:S(2)}) async-start(), calls=%async_computation.5 | async-start | bytes 4718592 | tf_op jit(solution)/shard_map/all_gather | solution.py:152
  41.3 221.0 %reduce-scatter.5.cloned.1.call-start = ((), (), s32[]{:S(2)}) async-start(), calls=%async_computation.8 | async-start | bytes 3276800 | tf_op jit(solution)/shard_map/reduce_scatter | solution.py:201
  46.9 12.0 %copy-start.12 = (bf16[1,2048,256]{2,1,0:T(8,128)(2,1)S(1)}, bf16[1,2048,256]{2,1,0:T(8,128)(2,1)}, u32[]{:S(2)}) copy-start(bf16[1,2048,256]{2,1,0:T(8,128)(2,1)} %param.29) | copy-start | bytes 3145732
  67.7 224.8 %reduce-scatter.3.cloned.1.call-start = ((), (), s32[]{:S(2)}) async-start(), calls=%async_computation.6 | async-start | bytes 1310720 | tf_op jit(solution)/shard_map/reduce_scatter | solution.py:185
  213.6 5.7 %copy-start.2 = (bf16[2,1024,1024]{2,1,0:T(8,128)(2,1)S(1)}, bf16[2,1024,1024]{2,1,0:T(8,128)(2,1)}, u32[]{:S(2)}) copy-start(bf16[2,1024,1024]{2,1,0:T(8,128)(2,1)} %get-tuple-element.211) | copy-start | bytes 12582916 | tf_op jit(solution)/shard_map/while
  238.1 5.0 %copy-start.2 = (bf16[2,1024,1024]{2,1,0:T(8,128)(2,1)S(1)}, bf16[2,1024,1024]{2,1,0:T(8,128)(2,1)}, u32[]{:S(2)}) copy-start(bf16[2,1024,1024]{2,1,0:T(8,128)(2,1)} %get-tuple-element.211) | copy-start | bytes 12582916 | tf_op jit(solution)/shard_map/while
  257.0 0.7 copy-start.8
  257.7 0.7 copy-start.9
  257.7 2.2 copy-start.11
  264.1 9.0 %copy-start.6 = (s32[64]{0:T(128)S(1)}, s32[64]{0:T(128)}, u32[]{:S(2)}) copy-start(s32[64]{0:T(128)} %copy-done.5) | copy-start | bytes 772
  264.1 9.1 %copy-start.7 = (s32[128,2]{0,1:T(2,128)S(1)}, s32[128,2]{0,1:T(2,128)}, u32[]{:S(2)}) copy-start(s32[128,2]{0,1:T(2,128)} %param.26) | copy-start | bytes 3076
  264.1 9.5 %copy-start.10 = (f32[128,2]{0,1:T(2,128)S(1)}, f32[128,2]{0,1:T(2,128)}, u32[]{:S(2)}) copy-start(f32[128,2]{0,1:T(2,128)} %param.27) | copy-start | bytes 3076
  269.6 17.8 %all-to-all-start.1 = ((bf16[8,2,16384]{2,1,0:T(2,128)(2,1)}), bf16[8,2,16384]{2,1,0:T(2,128)(2,1)S(1)}, u32[]{:S(2)}, u32[]{:S(2)}) async-start(bf16[8,2,16384]{2,1,0:T(2,128)(2,1)} %reshape.361), calls=%async_computation.3 | async-start | bytes 1048576 | tf_op jit(solution)/shard_map/all_to_all | solution.py:213
  287.9 4.6 %copy-start.1 = (bf16[1,256,2048]{2,1,0:T(8,128)(2,1)S(1)}, bf16[1,256,2048]{2,1,0:T(8,128)(2,1)}, u32[]{:S(2)}) copy-start(bf16[1,256,2048]{2,1,0:T(8,128)(2,1)} %param.30) | copy-start | bytes 3145732
Sparse Core Ops, SparseCore 0:
  34.7 21.5 all-gather.7
  58.4 74.6 all-gather.3
  135.2 70.9 all-gather.5
  208.6 33.0 reduce-scatter.4
  262.3 23.6 reduce-scatter.2
where the time goes:
time: 300 us; the launch traced here: 299 us
  waiting for transfers between devices  157 us (52%)
  matrix products  39.2 us (13%)
  local copies, waits for them, and re-layouts  32.9 us (11%)
  other arithmetic  29.7 us (10%)
  blocking collectives  21.7 us (7%)
  between operations  14.2 us (5%)
  starting transfers between devices  3.87 us (1%)
    all_gather x1, waiting for transfers between devices, local(): lax.all_gather(value_rows, 'ep', axis=0, tiled=True)  68.5 us
    all_gather x1, waiting for transfers between devices, local(): lax.all_gather(rot_keys, 'ep', axis=0, tiled=True)  65.1 us
    all_to_all x1, blocking collectives, local(): lax.all_to_all(outgoing[:, None], 'ep', split_axis=0, concat_axis=2, tile...  21.7 us
    dot_general x2, matrix products, one_block(): jnp.einsum('hmqk,khe->hmqe', weights.astype(jnp.bfloat16), value_view, pr...  14.4 us
    all_to_all x1, waiting for transfers between devices, local(): lax.all_to_all(routed, 'ep', split_axis=1, concat_axis=0, tiled=True)  13.5 us
    dynamic_slice x6, local copies, waits for them, and re-layouts, fold_keys(): result, _ = lax.scan(one_block, state_in, blocks)  12.4 us
    dot_general x2, matrix products, one_block(): jnp.einsum('qhmd,khmd->hmqk', query_view, key_view, preferred_element_typ...  11.2 us
    reduce_sum x2, other arithmetic, one_block(): denominator = denominator * shrink + jnp.sum(weights, axis=-1)  10.6 us
  transfers between devices with their start and end apart: 6, of which 4 were waited for; matrix products, arithmetic and copies ran while one was open for 31% of the time, Pallas kernels for 0%

commit v1 on v0

v1 whole, which is shorter than its diff:
```python
import jax
import jax.numpy as jnp
from jax import lax
from jax.experimental import pallas as pl
from jax.experimental.pallas import tpu as pltpu
from jax.sharding import PartitionSpec as P

theta_base = 500000.0
norm_eps = 1e-06
head_eps = 1e-05


def rms_rows(values, gain):
    widened = values.astype(jnp.float32)
    mean_square = jnp.mean(widened * widened, axis=-1, keepdims=True)
    return (widened * lax.rsqrt(mean_square + norm_eps) * gain).astype(jnp.bfloat16)


def gated_hidden(rows_in, gate_weight, up_weight):
    gate_part = jnp.dot(rows_in, gate_weight, preferred_element_type=jnp.float32)
    up_part = jnp.dot(rows_in, up_weight, preferred_element_type=jnp.float32)
    return (jax.nn.silu(gate_part) * up_part).astype(jnp.bfloat16)


def swap(pieces, axis):
    count = len(pieces)
    if count <= 8:
        return [pieces[0]] + [
            lax.ppermute(pieces[s], axis, [(j, j ^ s) for j in range(count)])
            for s in range(1, count)
        ]
    order = lax.axis_index(axis) ^ jnp.arange(count, dtype=jnp.int32)
    natural = jnp.take(jnp.stack(pieces), order, axis=0)
    moved = lax.all_to_all(natural, axis, split_axis=0, concat_axis=0, tiled=True)
    return list(jnp.take(moved, order, axis=0))


def rotate_call(queries, key_rows, value_rows, cosine, sines, place, head_count, head_dim):
    rows = queries.shape[0]
    width = 2 * head_dim

    def kernel(place_ref, q_ref, k_ref, v_ref, cos_ref, sin_ref, *outs):
        cosine = cos_ref[...]
        sines = sin_ref[...]
        for s in range(head_count):
            base = pl.multiple_of(((place_ref[0] ^ s) % head_count) * width, width)
            for ref, out in ((k_ref, outs[head_count + s]), (q_ref, outs[s])):
                for m in range(2):
                    part = ref[:, pl.ds(base + m * head_dim, head_dim)].astype(jnp.float32)
                    turned = part * cosine + pltpu.roll(part, head_dim // 2, 1) * sines
                    out[:, m * head_dim : (m + 1) * head_dim] = turned.astype(jnp.bfloat16)
            outs[2 * head_count + s][...] = v_ref[:, pl.ds(base, width)]

    vmem = pl.BlockSpec(memory_space=pltpu.VMEM)
    outs = pl.pallas_call(
        kernel,
        out_shape=[jax.ShapeDtypeStruct((rows, width), jnp.bfloat16)] * (3 * head_count),
        in_specs=[pl.BlockSpec(memory_space=pltpu.SMEM)] + [vmem] * 5,
        out_specs=[vmem] * (3 * head_count),
        cost_estimate=pl.CostEstimate(flops=rows * width * 100, transcendentals=0, bytes_accessed=rows * width * 48),
        name="rotate_split",
    )(place, queries, key_rows, value_rows, cosine, sines)
    return outs[:head_count], outs[head_count : 2 * head_count], outs[2 * head_count :]


def attend_call(q_parts, k_parts, v_parts, lam, head_gain, head_dim):
    rows, width = q_parts[0].shape
    n_q = len(q_parts)
    n_k = len(k_parts)
    factor = head_dim ** (-0.5) * 1.4426950408889634

    def kernel(lam_ref, gain_ref, *refs):
        q_refs = refs[:n_q]
        k_refs = refs[n_q : n_q + n_k]
        v_refs = refs[n_q + n_k : n_q + 2 * n_k]
        o_refs = refs[n_q + 2 * n_k : 2 * n_q + 2 * n_k]
        q_all, o_all = refs[2 * n_q + 2 * n_k :]
        for i in range(n_q):
            q_all[i] = q_refs[i][...]

        def one(i, carry):
            ratios = []
            for m in range(2):
                cols = slice(m * head_dim, (m + 1) * head_dim)
                query = q_all[i, :, cols]
                scores = [
                    lax.dot_general(
                        query, k[:, cols], (((1,), (1,)), ((), ())),
                        preferred_element_type=jnp.float32,
                    )
                    for k in k_refs
                ]
                top = scores[0]
                for part in scores[1:]:
                    top = jnp.maximum(top, part)
                top = jnp.max(top, axis=-1, keepdims=True)
                total = None
                weighted = None
                for part, v in zip(scores, v_refs):
                    weights = jnp.exp2((part - top) * factor)
                    total = weights if total is None else total + weights
                    product = jnp.dot(
                        weights.astype(jnp.bfloat16), v[...], preferred_element_type=jnp.float32
                    )
                    weighted = product if weighted is None else weighted + product
                ratios.append(weighted / jnp.sum(total, axis=-1, keepdims=True))
            mixed = ratios[0] - lam_ref[0] * ratios[1]
            mean_square = jnp.mean(mixed * mixed, axis=-1, keepdims=True)
            o_all[i] = (mixed * lax.rsqrt(mean_square + head_eps) * gain_ref[...]).astype(jnp.bfloat16)
            return carry

        lax.fori_loop(0, n_q, one, 0)
        for i in range(n_q):
            o_refs[i][...] = o_all[i]

    vmem = pl.BlockSpec(memory_space=pltpu.VMEM)
    return pl.pallas_call(
        kernel,
        out_shape=[jax.ShapeDtypeStruct((rows, width), jnp.bfloat16)] * n_q,
        in_specs=[pl.BlockSpec(memory_space=pltpu.SMEM)] + [vmem] * (1 + n_q + 2 * n_k),
        out_specs=[vmem] * n_q,
        scratch_shapes=[pltpu.VMEM((n_q, rows, width), jnp.bfloat16)] * 2,
        cost_estimate=pl.CostEstimate(
            flops=n_q * n_k * rows * rows * width * 6,
            transcendentals=n_q * n_k * rows * rows * 2,
            bytes_accessed=(n_q + n_k) * rows * width * 4,
        ),
        name="attend",
    )(lam, head_gain, *q_parts, *k_parts, *v_parts)


def project_call(parts, weight, places, tp_count):
    rows, width = parts[0].shape
    head_count = len(parts)
    wide = weight.shape[1]
    share = rows // tp_count

    def kernel(places_ref, *refs):
        o_refs = refs[:head_count]
        w_ref = refs[head_count]
        outs = refs[head_count + 1 : head_count + 1 + tp_count]
        scratch = refs[-1]
        total = None
        for s in range(head_count):
            base = pl.multiple_of(((places_ref[0] ^ s) % head_count) * width, width)
            product = jnp.dot(
                o_refs[s][...], w_ref[pl.ds(base, width), :], preferred_element_type=jnp.float32
            )
            total = product if total is None else total + product
        scratch[...] = total.astype(jnp.bfloat16)
        for u in range(tp_count):
            first = pl.multiple_of((places_ref[1] ^ u) * share, share)
            outs[u][...] = scratch[pl.ds(first, share), :]

    vmem = pl.BlockSpec(memory_space=pltpu.VMEM)
    return pl.pallas_call(
        kernel,
        out_shape=[jax.ShapeDtypeStruct((share, wide), jnp.bfloat16)] * tp_count,
        in_specs=[pl.BlockSpec(memory_space=pltpu.SMEM)] + [vmem] * (head_count + 1),
        out_specs=[vmem] * tp_count,
        scratch_shapes=[pltpu.VMEM((rows, wide), jnp.bfloat16)],
        cost_estimate=pl.CostEstimate(
            flops=2 * rows * width * head_count * wide,
            transcendentals=0,
            bytes_accessed=width * head_count * wide * 2 + rows * wide * 2,
        ),
        name="project",
    )(places, *parts, weight)


def slot_table(route_block, experts_order, capacity):
    flat_routes = route_block.reshape(-1)
    route_total = flat_routes.shape[0]
    top_count = route_block.shape[1]
    onehot = (flat_routes[:, None] == experts_order[None, :]).astype(jnp.int32)
    earlier = (
        jnp.arange(route_total)[:, None] > jnp.arange(route_total)[None, :]
    ) & (flat_routes[:, None] == flat_routes[None, :])
    slot_rank = jnp.sum(earlier.astype(jnp.int32), axis=1)
    slot_iota = jnp.arange(capacity, dtype=jnp.int32)
    matches = (onehot.T[:, None, :] > 0) & (slot_rank[None, None, :] == slot_iota[None, :, None])
    pick = jnp.sum(
        matches.reshape(experts_order.shape[0] * capacity, route_total // top_count, top_count),
        axis=2,
    ).astype(jnp.bfloat16)
    return pick, slot_rank.reshape(route_block.shape)


def local(
    queries,
    key_rows,
    value_rows,
    lambdas,
    head_gain,
    out_proj,
    moe_input,
    moe_gain,
    routes,
    route_weights,
    expert_gate,
    expert_up,
    expert_down,
    shared_gate,
    shared_up,
    shared_down,
):
    query_rows = queries.shape[0]
    head_count = lambdas.shape[0]
    head_dim = queries.shape[1] // (2 * head_count)
    tp_count = lax.axis_size("tp")
    ep_count = lax.axis_size("ep")
    tp_place = lax.axis_index("tp")
    ep_place = lax.axis_index("ep")
    places = jnp.stack([ep_place, tp_place]).astype(jnp.int32)

    batch_rows = moe_input.shape[0]
    top_count = routes.shape[1]
    own_rows = batch_rows // tp_count
    local_experts = expert_gate.shape[0]
    expert_count = local_experts * ep_count
    capacity = (2 * own_rows * top_count + expert_count - 1) // expert_count
    own_routes = lax.dynamic_slice_in_dim(routes, tp_place * own_rows, own_rows, 0)
    own_weights = lax.dynamic_slice_in_dim(route_weights, tp_place * own_rows, own_rows, 0)
    experts_order = (
        (ep_place ^ jnp.arange(ep_count, dtype=jnp.int32))[:, None] * local_experts
        + jnp.arange(local_experts, dtype=jnp.int32)[None, :]
    ).reshape(-1)
    pick, own_rank = slot_table(own_routes, experts_order, capacity)
    tp_order = tp_place ^ jnp.arange(tp_count, dtype=jnp.int32)
    ordered = jnp.take(moe_input.reshape(tp_count, own_rows, -1), tp_order, axis=0)
    normed = rms_rows(ordered.reshape(batch_rows, -1), moe_gain)
    outgoing = jnp.dot(pick, normed[:own_rows], preferred_element_type=jnp.float32)
    outgoing = outgoing.astype(jnp.bfloat16).reshape(ep_count, local_experts * capacity, -1)
    arrived = jnp.stack(swap([outgoing[s] for s in range(ep_count)], "ep"))

    positions = (ep_place * query_rows + jnp.arange(query_rows, dtype=jnp.int32)).astype(jnp.float32)
    half_dim = head_dim // 2
    frequency = jnp.power(theta_base, -jnp.arange(half_dim, dtype=jnp.float32) * 2.0 / head_dim)
    angles = positions[:, None] * frequency[None, :]
    cosine = jnp.cos(angles)
    sines = jnp.sin(angles)
    q_parts, k_parts, v_parts = rotate_call(
        queries,
        key_rows,
        value_rows,
        jnp.concatenate([cosine, cosine], axis=1),
        jnp.concatenate([-sines, sines], axis=1),
        places,
        head_count,
        head_dim,
    )
    q_parts = [q_parts[0]] + [
        lax.ppermute(q_parts[s], "ep", [(j, j ^ s) for j in range(ep_count)])
        for s in range(1, head_count)
    ]
    k_parts = swap([k_parts[s % head_count] for s in range(ep_count)], "ep")
    v_parts = swap([v_parts[s % head_count] for s in range(ep_count)], "ep")
    own_lambda = lax.dynamic_slice_in_dim(lambdas, ep_place % head_count, 1, 0)

    shared_hidden = gated_hidden(normed, shared_gate, shared_up)
    shared_part = jnp.dot(shared_hidden, shared_down, preferred_element_type=jnp.float32)
    shared_part = shared_part.astype(jnp.bfloat16).reshape(tp_count, own_rows, -1)
    slot_rows = local_experts * ep_count * capacity
    arrived = arrived.reshape(slot_rows, -1)
    if tp_count == 4:
        cross = lax.ppermute(arrived, "tp", [(j, j ^ 2) for j in range(4)])
        side = lax.ppermute(arrived, "tp", [(j, j ^ 1) for j in range(4)])
        corner = lax.ppermute(cross, "tp", [(j, j ^ 1) for j in range(4)])
        gathered = jnp.stack([arrived, side, cross, corner])
    else:
        gathered = lax.all_gather(arrived, "tp", axis=0, tiled=False)
        gathered = jnp.take(gathered, tp_order, axis=0)
    slots = gathered.reshape(tp_count, ep_count, local_experts, capacity, -1)
    slots = jnp.transpose(slots, (2, 0, 1, 3, 4)).reshape(local_experts, tp_count * ep_count * capacity, -1)
    gate_part = jnp.einsum("xsd,xdf->xsf", slots, expert_gate, preferred_element_type=jnp.float32)
    up_part = jnp.einsum("xsd,xdf->xsf", slots, expert_up, preferred_element_type=jnp.float32)
    hidden = (jax.nn.silu(gate_part) * up_part).astype(jnp.bfloat16)
    routed_part = jnp.einsum("xsf,xfd->xsd", hidden, expert_down, preferred_element_type=jnp.float32)
    routed_part = routed_part.astype(jnp.bfloat16).reshape(
        local_experts, tp_count, ep_count, capacity, -1
    )
    routed_part = jnp.transpose(routed_part, (1, 2, 0, 3, 4)).reshape(tp_count, slot_rows, -1)
    routed_got = swap([routed_part[u] for u in range(tp_count)], "tp")
    shared_got = swap([shared_part[u] for u in range(tp_count)], "tp")
    shared_sum = sum(part.astype(jnp.float32) for part in shared_got)
    routed = sum(part.astype(jnp.float32) for part in routed_got).astype(jnp.bfloat16)
    routed = routed.reshape(ep_count, local_experts * capacity, -1)
    returned = jnp.concatenate(swap([routed[s] for s in range(ep_count)], "ep"), axis=0)

    heads = attend_call(q_parts, k_parts, v_parts, own_lambda, head_gain[None, :], head_dim)
    heads = [heads[0]] + [
        lax.ppermute(heads[s], "ep", [(j, j ^ s) for j in range(ep_count)])
        for s in range(1, head_count)
    ]
    product = project_call(heads, out_proj, places, tp_count)
    mixer_out = sum(part.astype(jnp.float32) for part in swap(list(product), "tp"))
    mixer_out = mixer_out.astype(jnp.bfloat16)

    slot_of = (
        ((own_routes // local_experts) ^ ep_place) * local_experts + own_routes % local_experts
    ) * capacity + own_rank
    place_match = slot_of[:, :, None] == jnp.arange(slot_rows, dtype=jnp.int32)[None, None, :]
    combined = shared_sum
    for k in range(top_count):
        picked = jnp.dot(
            place_match[:, k].astype(jnp.bfloat16), returned, preferred_element_type=jnp.float32
        )
        combined = combined + own_weights[:, k : k + 1] * picked
    return (mixer_out, combined.astype(jnp.bfloat16))


def solution(mesh):
    in_specs = (
        P("ep", "tp"),
        P("ep", "tp"),
        P("ep", "tp"),
        P("tp"),
        P(),
        P("tp", None),
        P("ep", None),
        P(),
        P("ep", None),
        P("ep", None),
        P("ep", None, "tp"),
        P("ep", None, "tp"),
        P("ep", "tp", None),
        P(None, "tp"),
        P(None, "tp"),
        P("tp", None),
    )
    out_specs = (P(("ep", "tp"), None), P(("ep", "tp"), None))
    return jax.shard_map(local, mesh=mesh, in_specs=in_specs, out_specs=out_specs, check_vma=False)
```

time: 300 us -> 194 us (0.65)
  waiting for transfers between devices: 157 us -> 76.1 us
  starting transfers between devices: 3.87 us -> 65.2 us
  matrix products: 39.2 us -> 11.7 us
  other arithmetic: 29.7 us -> 7.76 us
  blocking collectives: 21.7 us -> 0 us
  local copies, waits for them, and re-layouts: 32.9 us -> 11.3 us
  Pallas kernels: 0 us -> 20.4 us
  between operations: 14.2 us -> 1.15 us
    all_gather x3 -> x0, waiting for transfers between devices: 143 us -> none  [the longest x1 68.5 us: local(): lax.all_gather(value_rows, 'ep', axis=0, tiled=True)]
    ppermute x0 -> x46, waiting for transfers between devices: none -> 76.1 us  [the longest x37 66.3 us: swap(): lax.ppermute(pieces[s], axis, [(j, j ^ s) for j in range(count)])]
    ppermute x0 -> x46, starting transfers between devices: none -> 65.2 us  [the longest x37 55.6 us: swap(): lax.ppermute(pieces[s], axis, [(j, j ^ s) for j in range(count)])]
    dot_general x7 -> x5, matrix products: 35.7 us -> 8.2 us  [the longest x1 4.3 us: local(): jnp.einsum('xsf,xfd->xsd', hidden, expert_down, preferred_element_type=jn...]
    all_to_all x1 -> x0, blocking collectives: 21.7 us -> none  [local(): lax.all_to_all(outgoing[:, None], 'ep', split_axis=0, concat_axis=2, tile...]
    pallas_call x0 -> x3, Pallas kernels: none -> 20.4 us  [the longest x1 12.6 us: attend_call(): pl.pallas_call(kernel, out_shape=[jax.ShapeDtypeStruct((rows, width), jnp...]
    all_to_all x1 -> x0, waiting for transfers between devices: 13.5 us -> none  [local(): lax.all_to_all(routed, 'ep', split_axis=1, concat_axis=0, tiled=True)]
    reduce_sum x6 -> x2, other arithmetic: 12.9 us -> 0.22 us  [the longest x1 0.18 us: slot_table(): slot_rank = jnp.sum(earlier.astype(jnp.int32), axis=1)]
  transfers between devices with their start and end apart: 6 -> 46, of which waited for: 4 -> 23; matrix products, arithmetic and copies ran while one was open for 31% -> 13% of each run, Pallas kernels for 0% -> 9%
where the time goes in v1:
time: 194 us
  waiting for transfers between devices  76.1 us (39%)
  starting transfers between devices  65.2 us (34%)
  Pallas kernels  20.4 us (11%)
  matrix products  11.7 us (6%)
  local copies, waits for them, and re-layouts  11.3 us (6%)
  other arithmetic  7.76 us (4%)
    ppermute x37, waiting for transfers between devices, swap(): lax.ppermute(pieces[s], axis, [(j, j ^ s) for j in range(count)])  66.3 us
    ppermute x37, starting transfers between devices, swap(): lax.ppermute(pieces[s], axis, [(j, j ^ s) for j in range(count)])  55.6 us
    pallas_call x1, Pallas kernels, attend_call(): pl.pallas_call(kernel, out_shape=[jax.ShapeDtypeStruct((rows, width), jnp...  12.6 us
    unnamed x66, local copies, waits for them, and re-layouts  6.44 us
    ppermute x3, waiting for transfers between devices, local(): lax.ppermute(heads[s], 'ep', [(j, j ^ s) for j in range(ep_count)])  6.39 us
    pallas_call x1, Pallas kernels, project_call(): pl.pallas_call(kernel, out_shape=[jax.ShapeDtypeStruct((share, wide), jnp...  4.7 us
    dot_general x1, matrix products, local(): jnp.einsum('xsf,xfd->xsd', hidden, expert_down, preferred_element_type=jn...  4.3 us
  transfers between devices with their start and end apart: 46, of which 23 were waited for; matrix products, arithmetic and copies ran while one was open for 13% of the time, Pallas kernels for 9%

profile of v1, /device:TPU:0, one launch (start us, length us, event | category | flops | bytes accessed | tf_op | source)
XLA Modules:
  0.0 193.6 jit_solution(14777708781138943481)
XLA Ops:
  2.7 3.1 %rotate_split.1 = (bf16[256,256]{1,0:T(8,128)(2,1)}, bf16[256,256]{1,0:T(8,128)(2,1)}, bf16[256,256]{1,0:T(8,128)(2,1)}, bf16[256,256]{1,0:T(8,128)(2,1)}, bf16[...) custom-call(s32[2]{0:T(128)} %pad_add_fusion.place_ref.places_ref, ...), custom_call_target="tpu_custom_call" | custom-call | flops 6553600 | bytes 3145728 | tf_op jit(solution)/shard_map/rotate_split/pallas_call | solution.py:55
  5.8 3.0 %collective-permute-start.10 = (bf16[256,256]{1,0:T(8,128)(2,1)}, bf16[256,256]{1,0:T(8,128)(2,1)}, u32[]{:S(2)}, u32[]{:S(2)}) collective-permute-start(bf16[256,256]{1,0:T(8,128)(2,1)} %get-tuple-element.31), channel_id=1, source_target_pairs={{0,4},{4,0},{8,12},{12,8},{16,20},{20,16},{24,28},{28,24},{1,5},{5... | collective-permute-start | bytes 393224 | tf_op jit(solution)/shard_map/ppermute | solution.py:29
  8.8 2.6 %collective-permute-start.14 = (bf16[256,256]{1,0:T(8,128)(2,1)}, bf16[256,256]{1,0:T(8,128)(2,1)}, u32[]{:S(2)}, u32[]{:S(2)}) collective-permute-start(bf16[256,256]{1,0:T(8,128)(2,1)} %get-tuple-element.31), channel_id=1, source_target_pairs={{0,20},{4,16},{8,28},{12,24},{16,4},{20,0},{24,12},{28,8},{1,21},{... | collective-permute-start | bytes 393224 | tf_op jit(solution)/shard_map/ppermute | solution.py:29
  22.2 3.0 %collective-permute-done.27 = bf16[16,2048]{1,0:T(8,128)(2,1)S(1)} collective-permute-done((bf16[16,2048]{1,0:T(8,128)(2,1)S(1)}, bf16[16,2048]{1,0:T(8,128)(2,1)S(1)}, u32[]{:S(2)}, u32[]{:S(2)}) %collective-permute-start.27) | collective-permute-done | bytes 65568 | tf_op jit(solution)/shard_map/ppermute | solution.py:29
  27.5 2.8 %collective-permute-done.28 = bf16[16,2048]{1,0:T(8,128)(2,1)S(1)} collective-permute-done((bf16[16,2048]{1,0:T(8,128)(2,1)S(1)}, bf16[16,2048]{1,0:T(8,128)(2,1)S(1)}, u32[]{:S(2)}, u32[]{:S(2)}) %collective-permute-start.28) | collective-permute-done | bytes 65568 | tf_op jit(solution)/shard_map/ppermute | solution.py:29
  30.4 2.4 %collective-permute-start.29 = (bf16[16,2048]{1,0:T(8,128)(2,1)S(1)}, bf16[16,2048]{1,0:T(8,128)(2,1)S(1)}, u32[]{:S(2)}, u32[]{:S(2)}) collective-permute-start(bf16[16,2048]{1,0:T(8,128)(2,1)S(1)} %get-tuple-element.59), channel_id=1, source_target_pairs={{0,16},{4,20},{8,24},{12,28},{16,0},{20,4},{24,8},{28,12},{1,17},{... | collective-permute-start | bytes 196616 | tf_op jit(solution)/shard_map/ppermute | solution.py:29
  33.4 4.0 %collective-permute-done.29 = bf16[16,2048]{1,0:T(8,128)(2,1)S(1)} collective-permute-done((bf16[16,2048]{1,0:T(8,128)(2,1)S(1)}, bf16[16,2048]{1,0:T(8,128)(2,1)S(1)}, u32[]{:S(2)}, u32[]{:S(2)}) %collective-permute-start.29) | collective-permute-done | bytes 65568 | tf_op jit(solution)/shard_map/ppermute | solution.py:29
  37.4 2.2 %collective-permute-start.30 = (bf16[16,2048]{1,0:T(8,128)(2,1)S(1)}, bf16[16,2048]{1,0:T(8,128)(2,1)S(1)}, u32[]{:S(2)}, u32[]{:S(2)}) collective-permute-start(bf16[16,2048]{1,0:T(8,128)(2,1)S(1)} %get-tuple-element.58), channel_id=1, source_target_pairs={{0,20},{4,16},{8,28},{12,24},{16,4},{20,0},{24,12},{28,8},{1,21},{... | collective-permute-start | bytes 196616 | tf_op jit(solution)/shard_map/ppermute | solution.py:29
  40.2 5.0 %collective-permute-done.30 = bf16[16,2048]{1,0:T(8,128)(2,1)S(1)} collective-permute-done((bf16[16,2048]{1,0:T(8,128)(2,1)S(1)}, bf16[16,2048]{1,0:T(8,128)(2,1)S(1)}, u32[]{:S(2)}, u32[]{:S(2)}) %collective-permute-start.30) | collective-permute-done | bytes 65568 | tf_op jit(solution)/shard_map/ppermute | solution.py:29
  45.2 2.9 %collective-permute-start.31 = (bf16[16,2048]{1,0:T(8,128)(2,1)S(1)}, bf16[16,2048]{1,0:T(8,128)(2,1)S(1)}, u32[]{:S(2)}, u32[]{:S(2)}) collective-permute-start(bf16[16,2048]{1,0:T(8,128)(2,1)S(1)} %get-tuple-element.57), channel_id=1, source_target_pairs={{0,24},{4,28},{8,16},{12,20},{16,8},{20,12},{24,0},{28,4},{1,25},{... | collective-permute-start | bytes 196616 | tf_op jit(solution)/shard_map/ppermute | solution.py:29
  48.7 2.6 %collective-permute-done.31 = bf16[16,2048]{1,0:T(8,128)(2,1)S(1)} collective-permute-done((bf16[16,2048]{1,0:T(8,128)(2,1)S(1)}, bf16[16,2048]{1,0:T(8,128)(2,1)S(1)}, u32[]{:S(2)}, u32[]{:S(2)}) %collective-permute-start.31) | collective-permute-done | bytes 65568 | tf_op jit(solution)/shard_map/ppermute | solution.py:29
  51.3 4.4 %collective-permute-start.32 = (bf16[16,2048]{1,0:T(8,128)(2,1)S(1)}, bf16[16,2048]{1,0:T(8,128)(2,1)S(1)}, u32[]{:S(2)}, u32[]{:S(2)}) collective-permute-start(bf16[16,2048]{1,0:T(8,128)(2,1)S(1)} %get-tuple-element.56), channel_id=1, source_target_pairs={{0,28},{4,24},{8,20},{12,16},{16,12},{20,8},{24,4},{28,0},{1,29},{... | collective-permute-start | bytes 196616 | tf_op jit(solution)/shard_map/ppermute | solution.py:29
  58.4 5.2 %collective-permute-start.13 = (bf16[256,256]{1,0:T(8,128)(2,1)S(1)}, bf16[256,256]{1,0:T(8,128)(2,1)S(1)}, u32[]{:S(2)}, u32[]{:S(2)}) collective-permute-start(bf16[256,256]{1,0:T(8,128)(2,1)S(1)} %copy-done.15), channel_id=1, source_target_pairs={{0,16},{4,20},{8,24},{12,28},{16,0},{20,4},{24,8},{28,12},{1,17},{... | collective-permute-start | bytes 393224 | tf_op jit(solution)/shard_map/ppermute | solution.py:29
  65.9 10.2 %collective-permute-done.13.refs_16_ = bf16[256,256]{1,0:T(8,128)(2,1)S(1)} collective-permute-done((bf16[256,256]{1,0:T(8,128)(2,1)S(1)}, bf16[256,256]{1,0:T(8,128)(2,1)S(1)}, u32[]{:S(2)}, u32[]{:S(2)}) %collective-permute-start.13) | collective-permute-done | bytes 131104 | tf_op jit(solution)/shard_map/ppermute | solution.py:29
  76.8 2.0 %collective-permute-start.34 = (bf16[128,2048]{1,0:T(8,128)(2,1)}, bf16[128,2048]{1,0:T(8,128)(2,1)}, u32[]{:S(2)}, u32[]{:S(2)}) collective-permute-start(bf16[128,2048]{1,0:T(8,128)(2,1)} %bitcast.17), channel_id=1, source_target_pairs={{0,2},{1,3},{2,0},{3,1},{4,6},{5,7},{6,4},{7,5},{8,10},{9,11},{10,... | collective-permute-start | bytes 1572872 | tf_op jit(solution)/shard_map/ppermute | solution.py:266
  78.8 2.0 %convolution_convert_fusion.2 = bf16[128,2048]{1,0:T(8,128)(2,1)S(1)} fusion(bf16[256,2048]{1,0:T(8,128)(2,1)S(1)} %copy-done.3, bf16[128,2048]{1,0:T(8,128)(2,1)S(1)} %multiply_convert_fusion, bf16[2048,256]{1,0:T(8,128)(2,1)} %param.30, f32[128,256]{1,0:T(8,128)S(1)} %fusion.32), kind=kOutput, calls=%fused_computation.4 | convolution fusion | flops 268894208 | bytes 3276800 | tf_op jit(solution)/shard_map/dot_general | solution.py:261
  82.1 2.4 %collective-permute-start.8 = (bf16[256,256]{1,0:T(8,128)(2,1)}, bf16[256,256]{1,0:T(8,128)(2,1)S(1)}, u32[]{:S(2)}, u32[]{:S(2)}) collective-permute-start(bf16[256,256]{1,0:T(8,128)(2,1)} %get-tuple-element.28), channel_id=1, source_target_pairs={{0,24},{4,28},{8,16},{12,20},{16,8},{20,12},{24,0},{28,4},{1,25},{... | collective-permute-start | bytes 393224 | tf_op jit(solution)/shard_map/ppermute | solution.py:29
  87.6 10.0 %collective-permute-done.6.refs_8_ = bf16[256,256]{1,0:T(8,128)(2,1)S(1)} collective-permute-done((bf16[256,256]{1,0:T(8,128)(2,1)S(1)}, bf16[256,256]{1,0:T(8,128)(2,1)S(1)}, u32[]{:S(2)}, u32[]{:S(2)}) %collective-permute-start.6) | collective-permute-done | bytes 131104 | tf_op jit(solution)/shard_map/ppermute | solution.py:29
  98.1 3.0 %collective-permute-start.2 = (bf16[256,256]{1,0:T(8,128)(2,1)}, bf16[256,256]{1,0:T(8,128)(2,1)}, u32[]{:S(2)}, u32[]{:S(2)}) collective-permute-start(bf16[256,256]{1,0:T(8,128)(2,1)} %get-tuple-element.25), channel_id=1, source_target_pairs={{0,12},{4,8},{8,4},{12,0},{16,28},{20,24},{24,20},{28,16},{1,13},{... | collective-permute-start | bytes 393224 | tf_op jit(solution)/shard_map/ppermute | solution.py:253
  103.4 2.4 %collective-permute-done.2.refs_3_ = bf16[256,256]{1,0:T(8,128)(2,1)} collective-permute-done((bf16[256,256]{1,0:T(8,128)(2,1)}, bf16[256,256]{1,0:T(8,128)(2,1)}, u32[]{:S(2)}, u32[]{:S(2)}) %collective-permute-start.2) | collective-permute-done | bytes 131104 | tf_op jit(solution)/shard_map/ppermute | solution.py:253
  105.9 12.6 %attend.1 = (bf16[256,256]{1,0:T(8,128)(2,1)}, bf16[256,256]{1,0:T(8,128)(2,1)}, bf16[256,256]{1,0:T(8,128)(2,1)}, bf16[256,256]{1,0:T(8,128)(2,1)}) custom-call(f32[1]{0:T(128)} %dynamic_slice.9.lam_ref, f32[1,256]{1,0:T(1,128)} %bitcast.86, bf16[256,256]{1,0:T(8,128)(2,1)} %get-tuple-element.22.refs_0_, bf16[256,256]{1,0:T(8,128)(2,1)} %copy-done.24, ...), custom_call_target="tpu_custom_call" | custom-call | flops 3221225472 | bytes 3145728 | tf_op jit(solution)/shard_map/attend/pallas_call | solution.py:117
  123.4 4.3 %fusion = bf16[1,512,2048]{2,1,0:T(8,128)(2,1)S(1)} fusion(bf16[1,256,2048]{2,1,0:T(8,128)(2,1)S(1)} %copy-done, f32[512,256]{1,0:T(8,128)} %fusion.6, bf16[512,2048]{1,0:T(8,128)(2,1)} %bitcast.82, bf16[1,2048,256]{2,1,0:T(8,128)(2,1)} %param.26), kind=kOutput, calls=%fused_computation.2 | convolution fusion | flops 1075576832 | bytes 6815744 | tf_op jit(solution)/shard_map/xsf,xfd->xsd/dot_general | solution.py:278
  134.1 3.2 %collective-permute-done.18.refs_2_ = bf16[256,256]{1,0:T(8,128)(2,1)S(1)} collective-permute-done((bf16[256,256]{1,0:T(8,128)(2,1)S(1)}, bf16[256,256]{1,0:T(8,128)(2,1)S(1)}, u32[]{:S(2)}, u32[]{:S(2)}) %collective-permute-start.18) | collective-permute-done | bytes 131104 | tf_op jit(solution)/shard_map/ppermute | solution.py:292
  137.4 3.2 %collective-permute-done.19.refs_3_ = bf16[256,256]{1,0:T(8,128)(2,1)S(1)} collective-permute-done((bf16[256,256]{1,0:T(8,128)(2,1)S(1)}, bf16[256,256]{1,0:T(8,128)(2,1)S(1)}, u32[]{:S(2)}, u32[]{:S(2)}) %collective-permute-start.19) | collective-permute-done | bytes 131104 | tf_op jit(solution)/shard_map/ppermute | solution.py:292
  141.8 4.7 %project.1 = (bf16[64,2048]{1,0:T(8,128)(2,1)}, bf16[64,2048]{1,0:T(8,128)(2,1)}, bf16[64,2048]{1,0:T(8,128)(2,1)}, bf16[64,2048]{1,0:T(8,128)(2,1)}) custom-call(s32[2]{0:T(128)} %pad_add_fusion.place_ref.places_ref, bf16[256,256]{1,0:T(8,128)(2,1)} %get-tuple-element.34.refs_0_, bf16[256,256]{1,0:T(8,128)(2,1)} %copy-done.6, bf16[256,256]{1,0:T(8,128)(2,1)} %copy-done.7, ...), custom_call_target="tpu_custom_call" | custom-call | flops 1073741824 | bytes 5242880 | tf_op jit(solution)/shard_map/project/pallas_call | solution.py:156
  147.4 7.0 %collective-permute-done.38 = bf16[128,2048]{1,0:T(8,128)(2,1)} collective-permute-done((bf16[128,2048]{1,0:T(8,128)(2,1)}, bf16[128,2048]{1,0:T(8,128)(2,1)}, u32[]{:S(2)}, u32[]{:S(2)}) %collective-permute-start.38) | collective-permute-done | bytes 524320 | tf_op jit(solution)/shard_map/ppermute | solution.py:29
  158.0 5.7 %collective-permute-done.21 = bf16[64,2048]{1,0:T(8,128)(2,1)S(1)} collective-permute-done((bf16[64,2048]{1,0:T(8,128)(2,1)}, bf16[64,2048]{1,0:T(8,128)(2,1)S(1)}, u32[]{:S(2)}, u32[]{:S(2)}) %collective-permute-start.21) | collective-permute-done | bytes 262176 | tf_op jit(solution)/shard_map/ppermute | solution.py:29
  165.2 3.1 %collective-permute-done.22 = bf16[64,2048]{1,0:T(8,128)(2,1)S(1)} collective-permute-done((bf16[64,2048]{1,0:T(8,128)(2,1)}, bf16[64,2048]{1,0:T(8,128)(2,1)S(1)}, u32[]{:S(2)}, u32[]{:S(2)}) %collective-permute-start.22) | collective-permute-done | bytes 262176 | tf_op jit(solution)/shard_map/ppermute | solution.py:29
  178.1 2.8 %collective-permute-done.42 = bf16[16,2048]{1,0:T(8,128)(2,1)S(1)} collective-permute-done((bf16[16,2048]{1,0:T(8,128)(2,1)S(1)}, bf16[16,2048]{1,0:T(8,128)(2,1)S(1)}, u32[]{:S(2)}, u32[]{:S(2)}) %collective-permute-start.42) | collective-permute-done | bytes 65568 | tf_op jit(solution)/shard_map/ppermute | solution.py:29
  180.9 3.5 %collective-permute-start.44 = (bf16[16,2048]{1,0:T(8,128)(2,1)S(1)}, bf16[16,2048]{1,0:T(8,128)(2,1)S(1)}, u32[]{:S(2)}, u32[]{:S(2)}) collective-permute-start(bf16[16,2048]{1,0:T(8,128)(2,1)S(1)} %get-tuple-element.49), channel_id=1, source_target_pairs={{0,24},{4,28},{8,16},{12,20},{16,8},{20,12},{24,0},{28,4},{1,25},{... | collective-permute-start | bytes 196616 | tf_op jit(solution)/shard_map/ppermute | solution.py:29
  184.4 2.4 %collective-permute-start.45 = (bf16[16,2048]{1,0:T(8,128)(2,1)S(1)}, bf16[16,2048]{1,0:T(8,128)(2,1)S(1)}, u32[]{:S(2)}, u32[]{:S(2)}) collective-permute-start(bf16[16,2048]{1,0:T(8,128)(2,1)S(1)} %get-tuple-element.48), channel_id=1, source_target_pairs={{0,28},{4,24},{8,20},{12,16},{16,12},{20,8},{24,4},{28,0},{1,29},{... | collective-permute-start | bytes 196616 | tf_op jit(solution)/shard_map/ppermute | solution.py:29
  186.9 4.5 %collective-permute-done.45 = bf16[16,2048]{1,0:T(8,128)(2,1)S(1)} collective-permute-done((bf16[16,2048]{1,0:T(8,128)(2,1)S(1)}, bf16[16,2048]{1,0:T(8,128)(2,1)S(1)}, u32[]{:S(2)}, u32[]{:S(2)}) %collective-permute-start.45) | collective-permute-done | bytes 65568 | tf_op jit(solution)/shard_map/ppermute | solution.py:29
  (177 shorter events, 60.2 us)
Async XLA Ops:
  5.8 52.5 %collective-permute-start.10 = (bf16[256,256]{1,0:T(8,128)(2,1)}, bf16[256,256]{1,0:T(8,128)(2,1)}, u32[]{:S(2)}, u32[]{:S(2)}) collective-permute-start(bf16[256,256]{1,0:T(8,128)(2,1)} %get-tuple-element.31), channel_id=1, source_target_pairs={{0,4},{4,0},{8,12},{12,8},{16,20},{20,16},{24,28},{28,24},{1,5},{5... | collective-permute-start | bytes 393224 | tf_op jit(solution)/shard_map/ppermute | solution.py:29
  8.8 67.3 %collective-permute-start.14 = (bf16[256,256]{1,0:T(8,128)(2,1)}, bf16[256,256]{1,0:T(8,128)(2,1)}, u32[]{:S(2)}, u32[]{:S(2)}) collective-permute-start(bf16[256,256]{1,0:T(8,128)(2,1)} %get-tuple-element.31), channel_id=1, source_target_pairs={{0,20},{4,16},{8,28},{12,24},{16,4},{20,0},{24,12},{28,8},{1,21},{... | collective-permute-start | bytes 393224 | tf_op jit(solution)/shard_map/ppermute | solution.py:29
  11.4 52.7 %collective-permute-start.11 = (bf16[256,256]{1,0:T(8,128)(2,1)}, bf16[256,256]{1,0:T(8,128)(2,1)}, u32[]{:S(2)}, u32[]{:S(2)}) collective-permute-start(bf16[256,256]{1,0:T(8,128)(2,1)} %get-tuple-element.32), channel_id=1, source_target_pairs={{0,8},{4,12},{8,0},{12,4},{16,24},{20,28},{24,16},{28,20},{1,9},{5... | collective-permute-start | bytes 393224 | tf_op jit(solution)/shard_map/ppermute | solution.py:29
  13.0 63.2 %collective-permute-start.15 = (bf16[256,256]{1,0:T(8,128)(2,1)}, bf16[256,256]{1,0:T(8,128)(2,1)}, u32[]{:S(2)}, u32[]{:S(2)}) collective-permute-start(bf16[256,256]{1,0:T(8,128)(2,1)} %get-tuple-element.32), channel_id=1, source_target_pairs={{0,24},{4,28},{8,16},{12,20},{16,8},{20,12},{24,0},{28,4},{1,25},{... | collective-permute-start | bytes 393224 | tf_op jit(solution)/shard_map/ppermute | solution.py:29
  37.4 7.8 %collective-permute-start.30 = (bf16[16,2048]{1,0:T(8,128)(2,1)S(1)}, bf16[16,2048]{1,0:T(8,128)(2,1)S(1)}, u32[]{:S(2)}, u32[]{:S(2)}) collective-permute-start(bf16[16,2048]{1,0:T(8,128)(2,1)S(1)} %get-tuple-element.58), channel_id=1, source_target_pairs={{0,20},{4,16},{8,28},{12,24},{16,4},{20,0},{24,12},{28,8},{1,21},{... | collective-permute-start | bytes 196616 | tf_op jit(solution)/shard_map/ppermute | solution.py:29
  51.3 7.1 %collective-permute-start.32 = (bf16[16,2048]{1,0:T(8,128)(2,1)S(1)}, bf16[16,2048]{1,0:T(8,128)(2,1)S(1)}, u32[]{:S(2)}, u32[]{:S(2)}) collective-permute-start(bf16[16,2048]{1,0:T(8,128)(2,1)S(1)} %get-tuple-element.56), channel_id=1, source_target_pairs={{0,28},{4,24},{8,20},{12,16},{16,12},{20,8},{24,4},{28,0},{1,29},{... | collective-permute-start | bytes 196616 | tf_op jit(solution)/shard_map/ppermute | solution.py:29
  58.4 17.8 %collective-permute-start.13 = (bf16[256,256]{1,0:T(8,128)(2,1)S(1)}, bf16[256,256]{1,0:T(8,128)(2,1)S(1)}, u32[]{:S(2)}, u32[]{:S(2)}) collective-permute-start(bf16[256,256]{1,0:T(8,128)(2,1)S(1)} %copy-done.15), channel_id=1, source_target_pairs={{0,16},{4,20},{8,24},{12,28},{16,0},{20,4},{24,8},{28,12},{1,17},{... | collective-permute-start | bytes 393224 | tf_op jit(solution)/shard_map/ppermute | solution.py:29
  64.1 16.7 %collective-permute-start.16 = (bf16[256,256]{1,0:T(8,128)(2,1)}, bf16[256,256]{1,0:T(8,128)(2,1)}, u32[]{:S(2)}, u32[]{:S(2)}) collective-permute-start(bf16[256,256]{1,0:T(8,128)(2,1)} %get-tuple-element.33), channel_id=1, source_target_pairs={{0,28},{4,24},{8,20},{12,16},{16,12},{20,8},{24,4},{28,0},{1,29},{... | collective-permute-start | bytes 393224 | tf_op jit(solution)/shard_map/ppermute | solution.py:29
  64.4 17.7 %collective-permute-start.3 = (bf16[256,256]{1,0:T(8,128)(2,1)}, bf16[256,256]{1,0:T(8,128)(2,1)}, u32[]{:S(2)}, u32[]{:S(2)}) collective-permute-start(bf16[256,256]{1,0:T(8,128)(2,1)} %get-tuple-element.27), channel_id=1, source_target_pairs={{0,4},{4,0},{8,12},{12,8},{16,20},{20,16},{24,28},{28,24},{1,5},{5... | collective-permute-start | bytes 393224 | tf_op jit(solution)/shard_map/ppermute | solution.py:29
  76.1 8.3 %collective-permute-start.4 = (bf16[256,256]{1,0:T(8,128)(2,1)}, bf16[256,256]{1,0:T(8,128)(2,1)}, u32[]{:S(2)}, u32[]{:S(2)}) collective-permute-start(bf16[256,256]{1,0:T(8,128)(2,1)} %get-tuple-element.28), channel_id=1, source_target_pairs={{0,8},{4,12},{8,0},{12,4},{16,24},{20,28},{24,16},{28,20},{1,9},{5... | collective-permute-start | bytes 393224 | tf_op jit(solution)/shard_map/ppermute | solution.py:29
  76.1 10.3 %collective-permute-start.5 = (bf16[256,256]{1,0:T(8,128)(2,1)}, bf16[256,256]{1,0:T(8,128)(2,1)}, u32[]{:S(2)}, u32[]{:S(2)}) collective-permute-start(bf16[256,256]{1,0:T(8,128)(2,1)} %get-tuple-element.29), channel_id=1, source_target_pairs={{0,12},{4,8},{8,4},{12,0},{16,28},{20,24},{24,20},{28,16},{1,13},{... | collective-permute-start | bytes 393224 | tf_op jit(solution)/shard_map/ppermute | solution.py:29
  76.8 24.4 %collective-permute-start.34 = (bf16[128,2048]{1,0:T(8,128)(2,1)}, bf16[128,2048]{1,0:T(8,128)(2,1)}, u32[]{:S(2)}, u32[]{:S(2)}) collective-permute-start(bf16[128,2048]{1,0:T(8,128)(2,1)} %bitcast.17), channel_id=1, source_target_pairs={{0,2},{1,3},{2,0},{3,1},{4,6},{5,7},{6,4},{7,5},{8,10},{9,11},{10,... | collective-permute-start | bytes 1572872 | tf_op jit(solution)/shard_map/ppermute | solution.py:266
  80.8 17.3 %collective-permute-start.7 = (bf16[256,256]{1,0:T(8,128)(2,1)}, bf16[256,256]{1,0:T(8,128)(2,1)S(1)}, u32[]{:S(2)}, u32[]{:S(2)}) collective-permute-start(bf16[256,256]{1,0:T(8,128)(2,1)} %get-tuple-element.27), channel_id=1, source_target_pairs={{0,20},{4,16},{8,28},{12,24},{16,4},{20,0},{24,12},{28,8},{1,21},{... | collective-permute-start | bytes 393224 | tf_op jit(solution)/shard_map/ppermute | solution.py:29
  82.1 16.0 %collective-permute-start.8 = (bf16[256,256]{1,0:T(8,128)(2,1)}, bf16[256,256]{1,0:T(8,128)(2,1)S(1)}, u32[]{:S(2)}, u32[]{:S(2)}) collective-permute-start(bf16[256,256]{1,0:T(8,128)(2,1)} %get-tuple-element.28), channel_id=1, source_target_pairs={{0,24},{4,28},{8,16},{12,20},{16,8},{20,12},{24,0},{28,4},{1,25},{... | collective-permute-start | bytes 393224 | tf_op jit(solution)/shard_map/ppermute | solution.py:29
  84.5 16.7 %collective-permute-start.9 = (bf16[256,256]{1,0:T(8,128)(2,1)}, bf16[256,256]{1,0:T(8,128)(2,1)S(1)}, u32[]{:S(2)}, u32[]{:S(2)}) collective-permute-start(bf16[256,256]{1,0:T(8,128)(2,1)} %get-tuple-element.29), channel_id=1, source_target_pairs={{0,28},{4,24},{8,20},{12,16},{16,12},{20,8},{24,4},{28,0},{1,29},{... | collective-permute-start | bytes 393224 | tf_op jit(solution)/shard_map/ppermute | solution.py:29
  86.4 11.3 %collective-permute-start.6 = (bf16[256,256]{1,0:T(8,128)(2,1)S(1)}, bf16[256,256]{1,0:T(8,128)(2,1)S(1)}, u32[]{:S(2)}, u32[]{:S(2)}) collective-permute-start(bf16[256,256]{1,0:T(8,128)(2,1)S(1)} %copy-done.14), channel_id=1, source_target_pairs={{0,16},{4,20},{8,24},{12,28},{16,0},{20,4},{24,8},{28,12},{1,17},{... | collective-permute-start | bytes 393224 | tf_op jit(solution)/shard_map/ppermute | solution.py:29
  98.1 7.7 %collective-permute-start.2 = (bf16[256,256]{1,0:T(8,128)(2,1)}, bf16[256,256]{1,0:T(8,128)(2,1)}, u32[]{:S(2)}, u32[]{:S(2)}) collective-permute-start(bf16[256,256]{1,0:T(8,128)(2,1)} %get-tuple-element.25), channel_id=1, source_target_pairs={{0,12},{4,8},{8,4},{12,0},{16,28},{20,24},{24,20},{28,16},{1,13},{... | collective-permute-start | bytes 393224 | tf_op jit(solution)/shard_map/ppermute | solution.py:253
  101.2 17.8 %collective-permute-start.33 = (bf16[128,2048]{1,0:T(8,128)(2,1)}, bf16[128,2048]{1,0:T(8,128)(2,1)S(1)}, u32[]{:S(2)}, u32[]{:S(2)}) collective-permute-start(bf16[128,2048]{1,0:T(8,128)(2,1)} %bitcast.17), channel_id=1, source_target_pairs={{0,1},{1,0},{2,3},{3,2},{4,5},{5,4},{6,7},{7,6},{8,9},{9,8},{10,11... | collective-permute-start | bytes 1572872 | tf_op jit(solution)/shard_map/ppermute | solution.py:267
  101.2 17.8 %collective-permute-start.35 = (bf16[128,2048]{1,0:T(8,128)(2,1)}, bf16[128,2048]{1,0:T(8,128)(2,1)S(1)}, u32[]{:S(2)}, u32[]{:S(2)}) collective-permute-start(bf16[128,2048]{1,0:T(8,128)(2,1)} %collective-permute-done.34), channel_id=1, source_target_pairs={{0,1},{1,0},{2,3},{3,2},{4,5},{5,4},{6,7},{7,6},{8,9},{9,8},{10,11... | collective-permute-start | bytes 1572872 | tf_op jit(solution)/shard_map/ppermute | solution.py:268
  118.5 14.2 %collective-permute-start.17 = (bf16[256,256]{1,0:T(8,128)(2,1)}, bf16[256,256]{1,0:T(8,128)(2,1)S(1)}, u32[]{:S(2)}, u32[]{:S(2)}) collective-permute-start(bf16[256,256]{1,0:T(8,128)(2,1)} %get-tuple-element.35), channel_id=1, source_target_pairs={{0,4},{4,0},{8,12},{12,8},{16,20},{20,16},{24,28},{28,24},{1,5},{5... | collective-permute-start | bytes 393224 | tf_op jit(solution)/shard_map/ppermute | solution.py:292
  128.9 17.5 %collective-permute-start.36 = (bf16[128,2048]{1,0:T(8,128)(2,1)}, bf16[128,2048]{1,0:T(8,128)(2,1)}, u32[]{:S(2)}, u32[]{:S(2)}) collective-permute-start(bf16[128,2048]{1,0:T(8,128)(2,1)} %get-tuple-element.42), channel_id=1, source_target_pairs={{0,1},{1,0},{2,3},{3,2},{4,5},{5,4},{6,7},{7,6},{8,9},{9,8},{10,11... | collective-permute-start | bytes 1572872 | tf_op jit(solution)/shard_map/ppermute | solution.py:29
  128.9 17.6 %collective-permute-start.37 = (bf16[128,2048]{1,0:T(8,128)(2,1)}, bf16[128,2048]{1,0:T(8,128)(2,1)}, u32[]{:S(2)}, u32[]{:S(2)}) collective-permute-start(bf16[128,2048]{1,0:T(8,128)(2,1)} %get-tuple-element.44), channel_id=1, source_target_pairs={{0,2},{1,3},{2,0},{3,1},{4,6},{5,7},{6,4},{7,5},{8,10},{9,11},{10,... | collective-permute-start | bytes 1572872 | tf_op jit(solution)/shard_map/ppermute | solution.py:29
  129.9 24.5 %collective-permute-start.38 = (bf16[128,2048]{1,0:T(8,128)(2,1)}, bf16[128,2048]{1,0:T(8,128)(2,1)}, u32[]{:S(2)}, u32[]{:S(2)}) collective-permute-start(bf16[128,2048]{1,0:T(8,128)(2,1)} %get-tuple-element.43), channel_id=1, source_target_pairs={{0,3},{1,2},{2,1},{3,0},{4,7},{5,6},{6,5},{7,4},{8,11},{9,10},{10,... | collective-permute-start | bytes 1572872 | tf_op jit(solution)/shard_map/ppermute | solution.py:29
  132.7 7.9 %collective-permute-start.19 = (bf16[256,256]{1,0:T(8,128)(2,1)S(1)}, bf16[256,256]{1,0:T(8,128)(2,1)S(1)}, u32[]{:S(2)}, u32[]{:S(2)}) collective-permute-start(bf16[256,256]{1,0:T(8,128)(2,1)S(1)} %copy-done.22), channel_id=1, source_target_pairs={{0,12},{4,8},{8,4},{12,0},{16,28},{20,24},{24,20},{28,16},{1,13},{... | collective-permute-start | bytes 393224 | tf_op jit(solution)/shard_map/ppermute | solution.py:292
  137.4 54.3 %collective-permute-start.23 = (bf16[32,2048]{1,0:T(8,128)(2,1)}, bf16[32,2048]{1,0:T(8,128)(2,1)}, u32[]{:S(2)}, u32[]{:S(2)}) collective-permute-start(bf16[32,2048]{1,0:T(8,128)(2,1)} %get-tuple-element.45), channel_id=1, source_target_pairs={{0,1},{1,0},{2,3},{3,2},{4,5},{5,4},{6,7},{7,6},{8,9},{9,8},{10,11... | collective-permute-start | bytes 393224 | tf_op jit(solution)/shard_map/ppermute | solution.py:29
  140.5 51.2 %collective-permute-start.24 = (bf16[32,2048]{1,0:T(8,128)(2,1)}, bf16[32,2048]{1,0:T(8,128)(2,1)}, u32[]{:S(2)}, u32[]{:S(2)}) collective-permute-start(bf16[32,2048]{1,0:T(8,128)(2,1)} %get-tuple-element.47), channel_id=1, source_target_pairs={{0,2},{1,3},{2,0},{3,1},{4,6},{5,7},{6,4},{7,5},{8,10},{9,11},{10,... | collective-permute-start | bytes 393224 | tf_op jit(solution)/shard_map/ppermute | solution.py:29
  146.5 11.0 %collective-permute-start.20 = (bf16[64,2048]{1,0:T(8,128)(2,1)}, bf16[64,2048]{1,0:T(8,128)(2,1)S(1)}, u32[]{:S(2)}, u32[]{:S(2)}) collective-permute-start(bf16[64,2048]{1,0:T(8,128)(2,1)} %get-tuple-element.39), channel_id=1, source_target_pairs={{0,1},{1,0},{2,3},{3,2},{4,5},{5,4},{6,7},{7,6},{8,9},{9,8},{10,11... | collective-permute-start | bytes 786440 | tf_op jit(solution)/shard_map/ppermute | solution.py:29
  146.6 17.1 %collective-permute-start.21 = (bf16[64,2048]{1,0:T(8,128)(2,1)}, bf16[64,2048]{1,0:T(8,128)(2,1)S(1)}, u32[]{:S(2)}, u32[]{:S(2)}) collective-permute-start(bf16[64,2048]{1,0:T(8,128)(2,1)} %get-tuple-element.40), channel_id=1, source_target_pairs={{0,2},{1,3},{2,0},{3,1},{4,6},{5,7},{6,4},{7,5},{8,10},{9,11},{10,... | collective-permute-start | bytes 786440 | tf_op jit(solution)/shard_map/ppermute | solution.py:29
  154.4 13.9 %collective-permute-start.22 = (bf16[64,2048]{1,0:T(8,128)(2,1)}, bf16[64,2048]{1,0:T(8,128)(2,1)S(1)}, u32[]{:S(2)}, u32[]{:S(2)}) collective-permute-start(bf16[64,2048]{1,0:T(8,128)(2,1)} %get-tuple-element.41), channel_id=1, source_target_pairs={{0,3},{1,2},{2,1},{3,0},{4,7},{5,6},{6,5},{7,4},{8,11},{9,10},{10,... | collective-permute-start | bytes 786440 | tf_op jit(solution)/shard_map/ppermute | solution.py:29
  157.4 34.2 %collective-permute-start.25 = (bf16[32,2048]{1,0:T(8,128)(2,1)S(1)}, bf16[32,2048]{1,0:T(8,128)(2,1)S(1)}, u32[]{:S(2)}, u32[]{:S(2)}) collective-permute-start(bf16[32,2048]{1,0:T(8,128)(2,1)S(1)} %copy-done.9), channel_id=1, source_target_pairs={{0,3},{1,2},{2,1},{3,0},{4,7},{5,6},{6,5},{7,4},{8,11},{9,10},{10,... | collective-permute-start | bytes 393224 | tf_op jit(solution)/shard_map/ppermute | solution.py:29
  163.6 7.2 %collective-permute-start.39 = (bf16[16,2048]{1,0:T(8,128)(2,1)S(1)}, bf16[16,2048]{1,0:T(8,128)(2,1)S(1)}, u32[]{:S(2)}, u32[]{:S(2)}) collective-permute-start(bf16[16,2048]{1,0:T(8,128)(2,1)S(1)} %get-tuple-element.54), channel_id=1, source_target_pairs={{0,4},{4,0},{8,12},{12,8},{16,20},{20,16},{24,28},{28,24},{1,5},{5... | collective-permute-start | bytes 196616 | tf_op jit(solution)/shard_map/ppermute | solution.py:29
  176.6 7.9 %collective-permute-start.43 = (bf16[16,2048]{1,0:T(8,128)(2,1)S(1)}, bf16[16,2048]{1,0:T(8,128)(2,1)S(1)}, u32[]{:S(2)}, u32[]{:S(2)}) collective-permute-start(bf16[16,2048]{1,0:T(8,128)(2,1)S(1)} %get-tuple-element.50), channel_id=1, source_target_pairs={{0,20},{4,16},{8,28},{12,24},{16,4},{20,0},{24,12},{28,8},{1,21},{... | collective-permute-start | bytes 196616 | tf_op jit(solution)/shard_map/ppermute | solution.py:29
  (40 other events, 594.5 us)
